TPU v7x, 32 devices: a whole 2x2x4 slice. The times are simulated.
32 devices in a mesh: sp: 8 (over z, y), dp: 4 (over x, core).
Axes of the slice: x: 2, y: 2, z: 4, core: 2. Of those that a mesh axis runs over, the one named last changes fastest.
Arguments:
- queries: bfloat16 [4, 1024, 2048], P('dp', 'sp'), may hold values from -40 to 40
- keys: bfloat16 [4, 1024, 512], P('dp', 'sp'), may hold values from -8 to 8
- values: bfloat16 [4, 1024, 512], P('dp', 'sp'), may hold values from -6 to 6
- lambdas: float32 [16], replicated, may hold values from 0.3 to 0.8
- value_gain: float32 [128], replicated, may hold values from 0.1 to 1.9
- out_weight: bfloat16 [2048, 4096], P(None, ('sp', 'dp')), may hold values from -0.125 to 0.125
Outputs:
- mixed: bfloat16 [4, 1024, 4096], P('dp', 'sp')
All inputs are finite; a program needn't handle non-finite values.
Results may differ from a plain program's by a relative error of at most 0.0087.
Values may be sent and summed in bfloat16 or wider, within the bound.
A program may use at most 128 MiB of HBM per device.

v0:
```python
import jax
import jax.numpy as jnp
from jax import lax
from jax.sharding import PartitionSpec as P

HEADS = 16
KV_HEADS = 4
HEAD_DIM = 64
VALUE_DIM = 128


rope_base = 500000.0
output_scale = 0.8
norm_eps = 1e-05


def swapped(block, axis, distance):
    count = lax.axis_size(axis)
    route = []
    for low in range(count):
        high = low | 1 << distance
        if high != low and high < count:
            route += [(low, high), (high, low)]
    return lax.ppermute(block, axis, route)


def rotate(parts, positions):
    width = parts.shape[-1]
    half = width // 2
    freqs = rope_base ** (-jnp.arange(0, width, 2, dtype=jnp.float32) / width)
    angles = positions[:, None] * freqs[None, :]
    shape = (angles.shape[0],) + (1,) * (parts.ndim - 2) + (half,)
    cosine = jnp.cos(angles).reshape(shape)
    sine = jnp.sin(angles).reshape(shape)
    first = parts[..., :half]
    second = parts[..., half:]
    return jnp.concatenate([first * cosine - second * sine, second * cosine + first * sine], -1)


def gather_group(key_value, group_size):
    tok_rows = key_value.shape[0]
    sub_rows = tok_rows // group_size
    width = key_value.shape[-1]
    arranged = key_value.reshape(group_size, sub_rows, KV_HEADS, 2, width)
    arranged = jnp.transpose(arranged, (2, 0, 1, 3, 4)).reshape(
        group_size * KV_HEADS, sub_rows, 2, width
    )
    received = lax.all_to_all(arranged, "sp", split_axis=0, concat_axis=1, tiled=True)
    held = received.reshape(1, -1, sub_rows, 2, width)
    device_index = lax.axis_index("sp")
    for bit_number in range(group_size.bit_length() - 1):
        partner = swapped(held, "sp", bit_number)
        upper = device_index // 2**bit_number % 2 == 1
        held = jnp.concatenate(
            [jnp.where(upper, partner, held), jnp.where(upper, held, partner)], 0
        )
    ordered = jnp.transpose(held, (1, 0, 2, 3, 4)).reshape(-1, 2, width)
    return (ordered[:, 0], ordered[:, 1])


def attend(query_rot, key_rot, value_whole, lambda_heads, value_gain):
    seqlen = key_rot.shape[0]
    block_rows = min(512, seqlen)
    count = seqlen // block_rows
    score_scale = query_rot.shape[-1] ** (-0.5)
    outputs = []
    for block_index in range(count):
        start = block_index * block_rows
        reach = start + block_rows
        query_block = query_rot[start:reach]
        key_part = key_rot[:reach]
        value_part = value_whole[:reach]
        scores = (
            jnp.einsum("qhmd,kmd->hmqk", query_block, key_part, preferred_element_type=jnp.float32)
            * score_scale
        )
        allowed = jnp.arange(reach)[None, :] <= (start + jnp.arange(block_rows))[:, None]
        scores = jnp.where(allowed[None, None], scores, -jnp.inf)
        row_top = jnp.max(scores, -1, keepdims=True)
        raised = jnp.exp(scores - row_top)
        maps = raised / jnp.sum(raised, -1, keepdims=True)
        weights = (maps[:, 0] - lambda_heads[:, None, None] * maps[:, 1]).astype(jnp.bfloat16)
        outputs.append(
            jnp.einsum("hqk,ke->qhe", weights, value_part, preferred_element_type=jnp.float32)
        )
    head_values = jnp.concatenate(outputs, 0)
    squares = jnp.mean(head_values * head_values, -1, keepdims=True)
    normed = head_values * lax.rsqrt(squares + norm_eps) * value_gain * output_scale
    return normed.astype(jnp.bfloat16)


def shards(queries, keys, values, lambdas, value_gain, out_weight):
    tok_rows = queries.shape[1]
    sp_count = lax.axis_size("sp")
    group_size = sp_count // KV_HEADS
    per_device = HEADS // sp_count
    query_split = queries[0].reshape(tok_rows, HEADS, 2 * HEAD_DIM)
    key_split = keys[0].reshape(tok_rows, KV_HEADS, 2 * HEAD_DIM)
    value_split = values[0].reshape(tok_rows, KV_HEADS, VALUE_DIM)
    query_heads = lax.all_to_all(query_split, "sp", split_axis=1, concat_axis=0, tiled=True)
    key_whole, value_whole = gather_group(jnp.stack([key_split, value_split], 2), group_size)
    seqlen = query_heads.shape[0]
    positions = jnp.arange(seqlen, dtype=jnp.float32)
    query_rot = rotate(
        query_heads.reshape(seqlen, per_device, 2, HEAD_DIM).astype(jnp.float32), positions
    ).astype(jnp.bfloat16)
    key_rot = rotate(key_whole.reshape(seqlen, 2, HEAD_DIM).astype(jnp.float32), positions).astype(
        jnp.bfloat16
    )
    lambda_heads = lax.dynamic_slice_in_dim(
        lambdas, lax.axis_index("sp") * per_device, per_device, 0
    )
    head_out = attend(query_rot, key_rot, value_whole, lambda_heads, value_gain)
    heads_local = lax.all_to_all(
        head_out.reshape(seqlen, per_device * VALUE_DIM),
        "sp",
        split_axis=0,
        concat_axis=1,
        tiled=True,
    )
    mixed = jnp.dot(
        heads_local,
        lax.all_gather(out_weight, ("sp", "dp"), axis=1, tiled=True),
        preferred_element_type=jnp.float32,
    ).astype(jnp.bfloat16)
    return mixed[None]


def solution(mesh):
    return jax.shard_map(
        shards,
        mesh=mesh,
        in_specs=(
            P("dp", "sp", None),
            P("dp", "sp", None),
            P("dp", "sp", None),
            P(),
            P(),
            P(None, ("sp", "dp")),
        ),
        out_specs=P("dp", "sp", None),
        check_vma=False,
    )
```

profile of v0, /device:TPU:0, one launch (start us, length us, event | category | flops | bytes accessed | tf_op | source)
XLA Modules:
  0.0 182.8 jit_solution(17417908235289656183)
XLA Ops:
  6.5 0.0 copy-start
  6.5 0.0 copy-start.2
  6.5 0.0 all-gather.2.cloned.1.call-start
  6.5 0.7 all-gather.2.cloned.1.call-update
  7.3 0.9 stack.7
  8.2 0.9 stack.8
  9.2 0.7 pad_maximum_fusion.3
  9.9 7.3 %all-to-all-start = ((bf16[8,64,2,128]{3,1,2,0:T(8,128)(2,1)}), bf16[8,64,2,128]{3,1,2,0:T(8,128)(2,1)S(1)}, u32[]{:S(2)}, u32[]{:S(2)}) async-start(bf16[8,64,2,128]{3,1,2,0:T(8,128)(2,1)} %bitcast.1), calls=%async_computation | async-start | bytes 524288 | tf_op jit(solution)/shard_map/all_to_all | solution.py:48
  17.2 2.0 %copy.40 = bf16[1,128,2048]{1,2,0:T(8,128)(2,1)} copy(bf16[1,128,2048]{2,1,0:T(8,128)(2,1)} %param.6) | data formatting | bytes 1048576 | tf_op args[0]
  19.3 0.5 fusion.39
  19.8 0.4 iota_compare_fusion
  20.2 6.0 %all-to-all-done = bf16[8,64,2,128]{3,1,2,0:T(8,128)(2,1)S(1)} async-done(((bf16[8,64,2,128]{3,1,2,0:T(8,128)(2,1)}), bf16[8,64,2,128]{3,1,2,0:T(8,128)(2,1)S(1)}, u32[]{:S(2)}, u32[]{:S(2)}) %all-to-all-start) | async-done | bytes 262176 | tf_op jit(solution)/shard_map/all_to_all | solution.py:48
  26.3 3.5 %all-to-all-start.1 = ((bf16[128,16,128]{0,2,1:T(8,128)(2,1)}), bf16[128,16,128]{0,2,1:T(8,128)(2,1)S(1)}, u32[]{:S(2)}, u32[]{:S(2)}) async-start(bf16[128,16,128]{0,2,1:T(8,128)(2,1)} %bitcast.10), calls=%async_computation.1 | async-start | bytes 1048576 | tf_op jit(solution)/shard_map/all_to_all | solution.py:100
  29.8 2.0 %collective-permute-start = (bf16[1,8,64,2,128]{4,2,3,1,0:T(8,128)(2,1)S(1)}, bf16[1,8,64,2,128]{4,2,3,1,0:T(8,128)(2,1)S(1)}, u32[]{:S(2)}, u32[]{:S(2)}) collective-permute-start(bf16[1,8,64,2,128]{4,2,3,1,0:T(8,128)(2,1)S(1)} %bitcast.118), channel_id=1, source_target_pairs={{0,4},{4,0},{8,12},{12,8},{16,20},{20,16},{24,28},{28,24},{1,5},{5... | collective-permute-start | bytes 786440 | tf_op jit(solution)/shard_map/ppermute | solution.py:24
  31.8 0.0 copy-done
  31.8 0.8 iota_compare_fusion.1
  32.5 0.0 copy-done.2
  32.5 0.1 dynamic_slice.3
  32.6 13.4 %collective-permute-done = bf16[1,8,64,2,128]{4,2,3,1,0:T(8,128)(2,1)S(1)} collective-permute-done((bf16[1,8,64,2,128]{4,2,3,1,0:T(8,128)(2,1)S(1)}, bf16[1,8,64,2,128]{4,2,3,1,0:T(8,128)(2,1)S(1)}, u32[]{:S(2)}, u32[]{:S(2)}) %collective-permute-start) | collective-permute-done | bytes 262176 | tf_op jit(solution)/shard_map/ppermute | solution.py:24
  46.1 0.1 maximum_bitcast_fusion
  46.2 0.2 copy.39
  46.4 0.7 subtract_convert_fusion.1
  47.2 6.0 %all-to-all-done.1 = bf16[128,16,128]{0,2,1:T(8,128)(2,1)S(1)} async-done(((bf16[128,16,128]{0,2,1:T(8,128)(2,1)}), bf16[128,16,128]{0,2,1:T(8,128)(2,1)S(1)}, u32[]{:S(2)}, u32[]{:S(2)}) %all-to-all-start.1) | async-done | bytes 524320 | tf_op jit(solution)/shard_map/all_to_all | solution.py:100
  53.1 0.1 convert_element_type.55
  53.2 0.6 copy.42
  53.9 0.2 reshape.176
  54.0 0.1 fusion.63
  54.1 0.1 subtract_convert_fusion
  54.3 4.5 %fusion.69 = (f32[2,2,512]{2,0,1:T(2,128)S(1)}, f32[2,2,512,512]{2,3,0,1:T(8,128)}) fusion(pred[512,512]{0,1:T(8,128)(4,1)} %iota_compare_fusion.1, bf16[1024,2,32]{0,2,1:T(8,128)(2,1)S(1)} %get-tuple-element.9, bf16[1024,2,32]{0,2,1:T(8,128)(2,1)} %get-tuple-element.10, bf16[1024,2,2,32]{0,3,1,2:T(8,128)(2,1)S(1)} %get-tuple-element.5, ...), kind=kOutput, calls=%fused_computation.77 | convolution fusion | flops 139198976 | bytes 5251072 | tf_op jit(solution)/shard_map/sub | solution.py:80
  58.8 0.0 copy-start.1
  58.8 3.0 %broadcast_divide_fusion.1 = f32[2,2,512,512]{2,3,0,1:T(8,128)S(1)} fusion(f32[2,2,512,512]{2,3,0,1:T(8,128)} %get-tuple-element.18, f32[2,2,512]{2,0,1:T(2,128)S(1)} %get-tuple-element.17), kind=kLoop, calls=%fused_computation.22 | loop fusion | flops 1048576 | bytes 8396800 | tf_op jit(solution)/shard_map/div | solution.py:81
  61.9 0.4 fusion.19
  62.3 0.0 copy-done.1
  62.3 5.3 %fusion.64 = (f32[2,2,512]{2,0,1:T(2,128)S(1)}, f32[2,2,512,1024]{2,3,0,1:T(8,128)}) fusion(pred[512,1024]{0,1:T(8,128)(4,1)S(1)} %iota_compare_fusion, bf16[1024,2,32]{0,2,1:T(8,128)(2,1)S(1)} %copy-done.1, bf16[1024,2,32]{0,2,1:T(8,128)(2,1)S(1)} %get-tuple-element.9, bf16[1024,2,2,32]{0,3,1,2:T(8,128)(2,1)S(1)} %get-tuple-element.6, ...), kind=kOutput, calls=%fused_computation.76 | convolution fusion | flops 277873664 | bytes 9707520 | tf_op jit(solution)/shard_map/sub | solution.py:80
  67.6 4.5 %broadcast_divide_fusion = f32[2,2,512,1024]{2,3,0,1:T(8,128)S(1)} fusion(f32[2,2,512,1024]{2,3,0,1:T(8,128)} %get-tuple-element.16, f32[2,2,512]{2,0,1:T(2,128)S(1)} %get-tuple-element.15), kind=kLoop, calls=%fused_computation.11 | loop fusion | flops 2097152 | bytes 16785408 | tf_op jit(solution)/shard_map/div | solution.py:81
  72.1 0.6 fusion.15
  72.8 0.1 fusion.21
  72.9 0.1 mul.266
  73.0 0.2 copy.61
  73.2 0.4 copy.50
  73.6 0.2 copy.48
  73.8 0.2 copy.49
  74.0 0.1 pad_maximum_fusion
  74.1 0.2 multiply_convert_fusion
  74.3 32.6 %all_to_all.34 = bf16[8,128,256]{2,1,0:T(8,128)(2,1)S(1)} all-to-all(bf16[8,128,256]{2,1,0:T(8,128)(2,1)S(1)} %multiply_convert_fusion), channel_id=1, replica_groups=mesh['sp'=8,'dp'=4] {'sp'}, dimensions={0} | all-to-all | bytes 1048576 | tf_op jit(solution)/shard_map/all_to_all | solution.py:114
  106.9 0.3 copy.51
  107.2 59.7 %all-gather.2.cloned.1.call-done = bf16[2048,4096]{1,0:T(8,128)(2,1)} async-done(((bf16[2048,128]{1,0:T(8,128)(2,1)}), bf16[2048,4096]{1,0:T(8,128)(2,1)}) %all-gather.2.cloned.1.call-update) | async-done | bytes 16777232 | tf_op jit(solution)/shard_map/all_gather | solution.py:123
  166.8 9.1 %fusion.3 = bf16[1,128,4096]{2,1,0:T(8,128)(2,1)} fusion(bf16[128,2048]{0,1:T(8,128)(2,1)S(1)} %bitcast.112, bf16[2048,4096]{1,0:T(8,128)(2,1)} %all-gather.2.cloned.1.call-done), kind=kOutput, calls=%fused_computation.6 | convolution fusion | flops 2148007936 | bytes 18350080 | tf_op jit(solution)/shard_map/dot_general | solution.py:121
  (9 shorter events, 0.2 us)
Async XLA Ops:
  6.5 25.2 %copy-start = (f32[128]{0:T(128)S(1)}, f32[128]{0:T(128)}, u32[]{:S(2)}) copy-start(f32[128]{0:T(128)} %param.10) | copy-start | bytes 1540
  6.5 26.0 %copy-start.2 = (f32[16]{0:T(128)S(1)}, f32[16]{0:T(128)}, u32[]{:S(2)}) copy-start(f32[16]{0:T(128)} %param.9) | copy-start | bytes 196
  6.5 160.3 %all-gather.2.cloned.1.call-start = ((), (), s32[]{:S(2)}) async-start(), calls=%async_computation.3 | async-start | bytes 17301504 | tf_op jit(solution)/shard_map/all_gather | solution.py:123
  9.9 16.3 %all-to-all-start = ((bf16[8,64,2,128]{3,1,2,0:T(8,128)(2,1)}), bf16[8,64,2,128]{3,1,2,0:T(8,128)(2,1)S(1)}, u32[]{:S(2)}, u32[]{:S(2)}) async-start(bf16[8,64,2,128]{3,1,2,0:T(8,128)(2,1)} %bitcast.1), calls=%async_computation | async-start | bytes 524288 | tf_op jit(solution)/shard_map/all_to_all | solution.py:48
  26.3 26.9 %all-to-all-start.1 = ((bf16[128,16,128]{0,2,1:T(8,128)(2,1)}), bf16[128,16,128]{0,2,1:T(8,128)(2,1)S(1)}, u32[]{:S(2)}, u32[]{:S(2)}) async-start(bf16[128,16,128]{0,2,1:T(8,128)(2,1)} %bitcast.10), calls=%async_computation.1 | async-start | bytes 1048576 | tf_op jit(solution)/shard_map/all_to_all | solution.py:100
  29.8 16.3 %collective-permute-start = (bf16[1,8,64,2,128]{4,2,3,1,0:T(8,128)(2,1)S(1)}, bf16[1,8,64,2,128]{4,2,3,1,0:T(8,128)(2,1)S(1)}, u32[]{:S(2)}, u32[]{:S(2)}) collective-permute-start(bf16[1,8,64,2,128]{4,2,3,1,0:T(8,128)(2,1)S(1)} %bitcast.118), channel_id=1, source_target_pairs={{0,4},{4,0},{8,12},{12,8},{16,20},{20,16},{24,28},{28,24},{1,5},{5... | collective-permute-start | bytes 786440 | tf_op jit(solution)/shard_map/ppermute | solution.py:24
  58.8 3.5 %copy-start.1 = (bf16[1024,2,32]{0,2,1:T(8,128)(2,1)S(1)}, bf16[1024,2,32]{0,2,1:T(8,128)(2,1)}, u32[]{:S(2)}) copy-start(bf16[1024,2,32]{0,2,1:T(8,128)(2,1)} %get-tuple-element.10) | copy-start | bytes 393220
Sparse Core Ops, SparseCore 0:
  10.2 156.6 all-gather.1
where the time goes:
time: 183 us
  waiting for transfers between devices  85.8 us (47%)
  blocking collectives  32.6 us (18%)
  matrix products  20.1 us (11%)
  between operations  13.6 us (7%)
  starting transfers between devices  12.8 us (7%)
  other arithmetic  11.4 us (6%)
  local copies, waits for them, and re-layouts  6.52 us (4%)
    all_gather x1, waiting for transfers between devices, shards(): lax.all_gather(out_weight, ('sp', 'dp'), axis=1, tiled=True)  59.7 us
    all_to_all x1, blocking collectives, shards(): lax.all_to_all(head_out.reshape(seqlen, per_device * VALUE_DIM), 'sp', sp...  32.6 us
    ppermute x1, waiting for transfers between devices, swapped(): return lax.ppermute(block, axis, route)  13.4 us
    sub x2, matrix products, attend(): raised = jnp.exp(scores - row_top)  9.88 us
    dot_general x1, matrix products, shards(): jnp.dot(heads_local, lax.all_gather(out_weight, ('sp', 'dp'), axis=1, til...  9.12 us
    div x2, other arithmetic, attend(): maps = raised / jnp.sum(raised, -1, keepdims=True)  7.49 us
    all_to_all x1, starting transfers between devices, gather_group(): lax.all_to_all(arranged, 'sp', split_axis=0, concat_axis=1, tiled=True)  7.31 us
    all_to_all x1, waiting for transfers between devices, gather_group(): lax.all_to_all(arranged, 'sp', split_axis=0, concat_axis=1, tiled=True)  6.03 us
  transfers between devices with their start and end apart: 4, of which 4 were waited for; matrix products, arithmetic and copies ran while one was open for 16% of the time, Pallas kernels for 0%

commit v1 on v0

v1 whole, which is shorter than its diff:
```python
import functools

import jax
import jax.numpy as jnp
from jax import lax
from jax.experimental import pallas as pl
from jax.experimental.pallas import tpu as pltpu
from jax.sharding import PartitionSpec as P

HEADS = 16
KV_HEADS = 4
HEAD_DIM = 64
VALUE_DIM = 128
GROUP = HEADS // KV_HEADS

rope_base = 500000.0
output_scale = 0.8
norm_eps = 1e-05
MESH = pl.DeviceIdType.MESH


def tables(positions):
    freqs = rope_base ** (-jnp.arange(0, HEAD_DIM, 2, dtype=jnp.float32) / HEAD_DIM)
    angles = positions[:, None] * freqs[None, :]
    cosine, sine = jnp.cos(angles), jnp.sin(angles)
    return jnp.concatenate([cosine] * 4, -1), jnp.concatenate([-sine, sine, -sine, sine], -1)


def turn(block, cosine, sine):
    half = HEAD_DIM // 2
    lane = lax.broadcasted_iota(jnp.int32, block.shape, 1)
    other = jnp.where(
        lane % HEAD_DIM < half,
        pltpu.roll(block, block.shape[1] - half, 1),
        pltpu.roll(block, half, 1),
    )
    return block * cosine + other * sine


def prep_kernel(k_ref, v_ref, cos_ref, sin_ref, kv_ref):
    width = 2 * HEAD_DIM
    for g in range(KV_HEADS):
        cols = slice(g * width, (g + 1) * width)
        kv_ref[:, cols] = turn(
            k_ref[:, cols].astype(jnp.float32), cos_ref[...], sin_ref[...]
        ).astype(jnp.bfloat16)
    kv_ref[:, KV_HEADS * width :] = v_ref[...]


def attend_kernel(lam_ref, q_ref, k_ref, v_ref, cos_ref, sin_ref, gain_ref, out_ref):
    rows, seqlen = q_ref.shape[0], k_ref.shape[0]
    g = pl.program_id(0)
    width = 2 * HEAD_DIM
    start = lax.axis_index("sp") * rows
    allowed = lax.broadcasted_iota(jnp.int32, (rows, seqlen), 1) <= (
        start + lax.broadcasted_iota(jnp.int32, (rows, seqlen), 0)
    )
    lane = lax.broadcasted_iota(jnp.int32, (rows, width), 1)
    gain = gain_ref[...]
    for h in range(GROUP):
        cols = slice(h * width, (h + 1) * width)
        query = turn(q_ref[:, cols].astype(jnp.float32), cos_ref[...], sin_ref[...])
        query = query.astype(jnp.bfloat16).astype(jnp.float32) * HEAD_DIM**-0.5
        maps = []
        for m in range(2):
            own = (lane < HEAD_DIM) if m == 0 else (lane >= HEAD_DIM)
            part = jnp.where(own, query, 0.0).astype(jnp.bfloat16)
            scores = lax.dot_general(
                part, k_ref[...], (((1,), (1,)), ((), ())), preferred_element_type=jnp.float32
            )
            scores = jnp.where(allowed, scores, -1e30)
            raised = jnp.exp(scores - jnp.max(scores, -1, keepdims=True))
            maps.append((raised, 1.0 / jnp.sum(raised, -1, keepdims=True)))
        lam = lam_ref[g * GROUP + h]
        weights = (
            maps[0][0] * maps[0][1] - maps[1][0] * (lam * maps[1][1])
        ).astype(jnp.bfloat16)
        value = jnp.dot(weights, v_ref[...], preferred_element_type=jnp.float32)
        squares = jnp.mean(value * value, -1, keepdims=True)
        normed = value * lax.rsqrt(squares + norm_eps) * gain * output_scale
        out_ref[:, cols] = normed.astype(jnp.bfloat16)


def send(src, dst, send_sem, recv_sem, dp):
    return pltpu.make_async_remote_copy(
        src_ref=src,
        dst_ref=dst,
        send_sem=send_sem,
        recv_sem=recv_sem,
        device_id={"dp": dp},
        device_id_type=MESH,
    )


def exchange_kernel(count, heads_ref, all_ref, own_sem, send_sems, recv_sems, fs_sems, fr_sems):
    d = lax.axis_index("dp")
    half = count // 2
    x, core = d // 2, d % 2
    mate = x * 2 + 1 - core
    barrier = pltpu.get_barrier_semaphore()
    pl.semaphore_signal(barrier, inc=1, device_id={"dp": mate}, device_id_type=MESH)
    for k in range(1, half):
        pl.semaphore_signal(
            barrier, inc=1, device_id={"dp": (x + k) % half * 2 + core}, device_id_type=MESH
        )
    pl.semaphore_wait(barrier, half)
    copies = []
    for k in range(1, half):
        copies.append(
            send(heads_ref, all_ref.at[d], send_sems.at[k], recv_sems.at[k], (x + k) % half * 2 + core)
        )
        copies[-1].start()
    first = send(heads_ref, all_ref.at[d], send_sems.at[0], recv_sems.at[0], mate)
    first.start()
    local = pltpu.make_async_copy(heads_ref, all_ref.at[d], own_sem)
    local.start()
    forwards = []
    for k in range(1, half):
        slot = all_ref.at[(x + half - k) % half * 2 + core]
        copies[k - 1].wait_recv()
        forwards.append(send(slot, slot, fs_sems.at[k], fr_sems.at[k], mate))
        forwards[-1].start()
    local.wait()
    first.wait()
    for copy in copies:
        copy.wait_send()
    for copy in forwards:
        copy.wait()


def project_kernel(count, per, heads_ref, w_ref, out_ref, built, send_sems, recv_sems):
    d = lax.axis_index("dp")
    barrier = pltpu.get_barrier_semaphore()
    for k in range(1, count):
        pl.semaphore_signal(barrier, inc=1, device_id={"dp": (d + k) % count}, device_id_type=MESH)
    rows, depth = heads_ref.shape[1:]
    heads = heads_ref[...].reshape(count * rows, depth)
    chunks = out_ref.shape[0]
    copies = []
    for j in range(chunks):
        weight = jnp.concatenate([w_ref[j * per + i] for i in range(per)], -1)
        mixed = jnp.dot(heads, weight, preferred_element_type=jnp.float32).astype(jnp.bfloat16)
        built[j] = mixed.reshape(count, rows, -1)
        if j == 0:
            pl.semaphore_wait(barrier, count - 1)
        for k in range(1, count):
            copies.append(
                send(
                    built.at[j, (d + k) % count],
                    out_ref.at[j, d],
                    send_sems.at[j, k],
                    recv_sems.at[j, k],
                    (d + k) % count,
                )
            )
            copies[-1].start()
        out_ref[j, d] = built[j, d]
    for copy in copies:
        copy.wait()


def shards(queries, keys, values, lambdas, value_gain, out_weight):
    rows = queries.shape[1]
    sp_count = lax.axis_size("sp")
    dp_count = lax.axis_size("dp")
    seqlen = rows * sp_count
    width = 2 * HEAD_DIM
    vmem = pl.BlockSpec(memory_space=pltpu.VMEM)
    bf16 = jnp.bfloat16
    positions = (lax.axis_index("sp") * rows + jnp.arange(rows)).astype(jnp.float32)
    cosine, sine = tables(positions)

    kv = pl.pallas_call(
        prep_kernel,
        out_shape=jax.ShapeDtypeStruct((rows, 2 * KV_HEADS * width), bf16),
        in_specs=[vmem] * 4,
        out_specs=vmem,
        name="prep",
    )(keys[0], values[0], cosine, sine)
    kv_whole = lax.all_gather(kv, "sp", axis=0, tiled=True)
    kv_whole, out_weight = lax.optimization_barrier((kv_whole, out_weight))
    weights = lax.all_gather(out_weight, "sp", axis=0)

    heads = pl.pallas_call(
        attend_kernel,
        grid=(KV_HEADS,),
        out_shape=jax.ShapeDtypeStruct((rows, HEADS * VALUE_DIM), bf16),
        in_specs=[
            pl.BlockSpec(memory_space=pltpu.SMEM),
            pl.BlockSpec((rows, GROUP * width), lambda g: (0, g)),
            pl.BlockSpec((seqlen, width), lambda g: (0, g)),
            pl.BlockSpec((seqlen, VALUE_DIM), lambda g: (0, KV_HEADS + g)),
            pl.BlockSpec((rows, width), lambda g: (0, 0)),
            pl.BlockSpec((rows, width), lambda g: (0, 0)),
            pl.BlockSpec((1, VALUE_DIM), lambda g: (0, 0)),
        ],
        out_specs=pl.BlockSpec((rows, GROUP * VALUE_DIM), lambda g: (0, g)),
        cost_estimate=pl.CostEstimate(
            flops=3 * 10**9, bytes_accessed=4 * 2**20, transcendentals=4 * 2**20
        ),
        name="attend",
    )(lambdas, queries[0], kv_whole, kv_whole, cosine, sine, value_gain[None])

    half = dp_count // 2
    dma = pltpu.SemaphoreType.DMA
    heads_all = pl.pallas_call(
        functools.partial(exchange_kernel, dp_count),
        out_shape=jax.ShapeDtypeStruct((dp_count, rows, HEADS * VALUE_DIM), bf16),
        in_specs=[vmem],
        out_specs=vmem,
        scratch_shapes=[dma(())] + [dma((half,))] * 4,
        compiler_params=pltpu.CompilerParams(collective_id=0, has_side_effects=True),
        cost_estimate=pl.CostEstimate(flops=0, bytes_accessed=32 * 2**20, transcendentals=0),
        name="exchange",
    )(heads)

    own = out_weight.shape[1]
    depth = out_weight.shape[0]
    block = min(256, sp_count * own)
    if own % 128:
        weights = jnp.transpose(weights, (1, 0, 2)).reshape(depth, -1, block)
        weights = jnp.transpose(weights, (1, 0, 2))
    per = max(1, block // weights.shape[2])
    chunks = weights.shape[0] // per
    block = per * weights.shape[2]
    mixed = pl.pallas_call(
        functools.partial(project_kernel, dp_count, per),
        out_shape=jax.ShapeDtypeStruct((chunks, dp_count, rows, block), bf16),
        in_specs=[vmem] * 2,
        out_specs=vmem,
        scratch_shapes=[
            pltpu.VMEM((chunks, dp_count, rows, block), bf16),
            dma((chunks, dp_count)),
            dma((chunks, dp_count)),
        ],
        compiler_params=pltpu.CompilerParams(collective_id=1, has_side_effects=True),
        name="project",
    )(heads_all, weights)
    mixed = mixed.reshape(chunks, dp_count, rows, block // own, own)
    mixed = jnp.transpose(mixed, (2, 0, 3, 1, 4))
    return mixed.reshape(1, rows, -1)


def solution(mesh):
    return jax.shard_map(
        shards,
        mesh=mesh,
        in_specs=(
            P("dp", "sp", None),
            P("dp", "sp", None),
            P("dp", "sp", None),
            P(),
            P(),
            P(None, ("sp", "dp")),
        ),
        out_specs=P("dp", "sp", None),
        check_vma=False,
    )
```

time: 183 us -> 164 us (0.90)
  Pallas kernels: 0 us -> 51 us
  blocking collectives: 32.6 us -> 0 us
  matrix products: 20.1 us -> 0 us
  starting transfers between devices: 12.8 us -> 0.04 us
  other arithmetic: 11.4 us -> 1.15 us
  waiting for transfers between devices: 85.8 us -> 93.9 us
  local copies, waits for them, and re-layouts: 6.52 us -> 4.31 us
    pallas_call x0 -> x4, Pallas kernels: none -> 51 us  [the longest x1 18 us: shards(): pl.pallas_call(functools.partial(exchange_kernel, dp_count), out_shape=ja...]
    all_gather x1 -> x2, waiting for transfers between devices: 59.7 us -> 93.8 us  [the longest x1 51.9 us: shards(): kv_whole = lax.all_gather(kv, 'sp', axis=0, tiled=True)]
    all_to_all x1 -> x0, blocking collectives: 32.6 us -> none  [shards(): lax.all_to_all(head_out.reshape(seqlen, per_device * VALUE_DIM), 'sp', sp...]
    ppermute x1 -> x0, waiting for transfers between devices: 13.4 us -> none  [swapped(): return lax.ppermute(block, axis, route)]
    all_to_all x2 -> x0, waiting for transfers between devices: 12 us -> none  [the longest x1 6.03 us: gather_group(): lax.all_to_all(arranged, 'sp', split_axis=0, concat_axis=1, tiled=True)]
    all_to_all x2 -> x0, starting transfers between devices: 10.8 us -> none  [the longest x1 7.31 us: gather_group(): lax.all_to_all(arranged, 'sp', split_axis=0, concat_axis=1, tiled=True)]
    dot_general x3 -> x0, matrix products: 10.2 us -> none  [the longest x1 9.12 us: shards(): jnp.dot(heads_local, lax.all_gather(out_weight, ('sp', 'dp'), axis=1, til...]
    sub x2 -> x0, matrix products: 9.88 us -> none  [attend(): raised = jnp.exp(scores - row_top)]
  transfers between devices with their start and end apart: 4 -> 2, of which waited for: 4 -> 2; matrix products, arithmetic and copies ran while one was open for 16% -> 0% of each run, Pallas kernels for 0% -> 19%
where the time goes in v1:
time: 164 us
  waiting for transfers between devices  93.9 us (57%)
  Pallas kernels  51 us (31%)
  between operations  13.4 us (8%)
  local copies, waits for them, and re-layouts  4.31 us (3%)
    all_gather x1, waiting for transfers between devices, shards(): kv_whole = lax.all_gather(kv, 'sp', axis=0, tiled=True)  51.9 us
    all_gather x1, waiting for transfers between devices, shards(): weights = lax.all_gather(out_weight, 'sp', axis=0)  41.9 us
    pallas_call x1, Pallas kernels, shards(): pl.pallas_call(functools.partial(exchange_kernel, dp_count), out_shape=ja...  18 us
    pallas_call x1, Pallas kernels, shards(): pl.pallas_call(functools.partial(project_kernel, dp_count, per), out_shap...  17.6 us
    pallas_call x1, Pallas kernels, shards(): pl.pallas_call(attend_kernel, grid=(KV_HEADS,), out_shape=jax.ShapeDtypeS...  13.6 us
  transfers between devices with their start and end apart: 2, of which 2 were waited for; matrix products, arithmetic and copies ran while one was open for 0% of the time, Pallas kernels for 19%

profile of v1, /device:TPU:0, one launch (start us, length us, event | category | flops | bytes accessed | tf_op | source)
XLA Modules:
  0.0 163.8 jit_solution(11462071988099693977)
XLA Ops:
  6.5 0.0 all-gather.4.cloned.1.call-start
  6.6 0.3 fusion
  6.9 0.8 pad_maximum_fusion
  7.7 1.8 %prep.1 = bf16[128,1024]{1,0:T(8,128)(2,1)} custom-call(bf16[128,512]{1,0:T(8,128)(2,1)} %bitcast.10, bf16[128,512]{1,0:T(8,128)(2,1)} %bitcast.11, f32[128,128]{1,0:T(8,128)} %get-tuple-element.12.cos_ref, f32[128,128]{1,0:T(8,128)} %get-tuple-element.13.sin_ref), custom_call_target="tpu_custom_call" | custom-call | tf_op jit(solution)/shard_map/prep/pallas_call | solution.py:173
  9.6 0.0 all-gather.4.cloned.1.call-update
  9.6 0.0 all-gather.6.cloned.1.call-start
  9.6 51.9 %all-gather.4.cloned.1.call-done.k_ref.v_ref = bf16[1024,1024]{1,0:T(8,128)(2,1)} async-done(((bf16[128,1024]{1,0:T(8,128)(2,1)}), bf16[1024,1024]{1,0:T(8,128)(2,1)}) %all-gather.4.cloned.1.call-update) | async-done | bytes 2097168 | tf_op jit(solution)/shard_map/all_gather | solution.py:180
  61.5 0.0 all-gather.6.cloned.1.call-update
  61.6 13.6 %attend.1.heads_ref = bf16[128,2048]{1,0:T(8,128)(2,1)} custom-call(f32[16]{0:T(128)} %lam_ref.1, bf16[128,2048]{1,0:T(8,128)(2,1)} %bitcast.12, bf16[1024,1024]{1,0:T(8,128)(2,1)} %all-gather.4.cloned.1.call-done.k_ref.v_ref, bf16[1024,1024]{1,0:T(8,128)(2,1)} %all-gather.4.cloned.1.call-done.k_ref.v_ref, f32[128,128]{1,0:T(8,128)} %get-tuple-element.12.cos_ref, ...), custom_call_target="tpu_custom_call" | custom-call | flops 3000000000 | bytes 4194304 | tf_op jit(solution)/shard_map/attend/pallas_call | solution.py:184
  75.1 18.0 %exchange.1.heads_ref = bf16[4,128,2048]{2,1,0:T(8,128)(2,1)} custom-call(bf16[128,2048]{1,0:T(8,128)(2,1)} %attend.1.heads_ref), custom_call_target="tpu_custom_call" | custom-call | bytes 33554432 | tf_op jit(solution)/shard_map/exchange/pallas_call | solution.py:206
  93.1 41.9 %all-gather.6.cloned.1.call-done = bf16[16384,128]{1,0:T(8,128)(2,1)} async-done(((bf16[2048,128]{1,0:T(8,128)(2,1)}), bf16[16384,128]{1,0:T(8,128)(2,1)}) %all-gather.6.cloned.1.call-update) | async-done | bytes 4194320 | tf_op jit(solution)/shard_map/all_gather | solution.py:182
  135.0 17.6 %project.1 = bf16[4,4,128,256]{3,2,1,0:T(8,128)(2,1)} custom-call(bf16[4,128,2048]{2,1,0:T(8,128)(2,1)} %exchange.1.heads_ref, bf16[8,2048,128]{2,1,0:T(8,128)(2,1)} %bitcast.8), custom_call_target="tpu_custom_call" | custom-call | tf_op jit(solution)/shard_map/project/pallas_call | solution.py:226
  152.7 1.3 reshape.18
  154.0 1.4 copy.9
  155.4 1.6 reshape.19
  (2 shorter events, 0.0 us)
Async XLA Ops:
  6.5 55.0 %all-gather.4.cloned.1.call-start = ((), (), s32[]{:S(2)}) async-start(), calls=%async_computation | async-start | bytes 2359296 | tf_op jit(solution)/shard_map/all_gather | solution.py:180
  9.6 125.5 %all-gather.6.cloned.1.call-start = ((), (), s32[]{:S(2)}) async-start(), calls=%async_computation.1 | async-start | bytes 4718592 | tf_op jit(solution)/shard_map/all_gather | solution.py:182
Sparse Core Ops, SparseCore 0:
  9.7 51.7 all-gather.3
  63.7 71.3 all-gather.5

commit v2 on v1

v2 whole, which is shorter than its diff:
```python
import functools

import jax
import jax.numpy as jnp
from jax import lax
from jax.experimental import pallas as pl
from jax.experimental.pallas import tpu as pltpu
from jax.sharding import PartitionSpec as P

HEADS = 16
KV_HEADS = 4
HEAD_DIM = 64
VALUE_DIM = 128
GROUP = HEADS // KV_HEADS

rope_base = 500000.0
output_scale = 0.8
norm_eps = 1e-05
MESH = pl.DeviceIdType.MESH


def tables(positions):
    freqs = rope_base ** (-jnp.arange(0, HEAD_DIM, 2, dtype=jnp.float32) / HEAD_DIM)
    angles = positions[:, None] * freqs[None, :]
    cosine, sine = jnp.cos(angles), jnp.sin(angles)
    return jnp.concatenate([cosine] * 4, -1), jnp.concatenate([-sine, sine, -sine, sine], -1)


def turn(block, cosine, sine):
    half = HEAD_DIM // 2
    lane = lax.broadcasted_iota(jnp.int32, block.shape, 1)
    other = jnp.where(
        lane % HEAD_DIM < half,
        pltpu.roll(block, block.shape[1] - half, 1),
        pltpu.roll(block, half, 1),
    )
    return block * cosine + other * sine


def prep_kernel(k_ref, v_ref, cos_ref, sin_ref, kv_ref):
    width = 2 * HEAD_DIM
    for g in range(KV_HEADS):
        cols = slice(g * width, (g + 1) * width)
        kv_ref[:, cols] = turn(
            k_ref[:, cols].astype(jnp.float32), cos_ref[...], sin_ref[...]
        ).astype(jnp.bfloat16)
    kv_ref[:, KV_HEADS * width :] = v_ref[...]


def send(src, dst, send_sem, recv_sem, axis, index):
    return pltpu.make_async_remote_copy(
        src_ref=src,
        dst_ref=dst,
        send_sem=send_sem,
        recv_sem=recv_sem,
        device_id={axis: index},
        device_id_type=MESH,
    )


def layer_kernel(
    n,
    count,
    lam_ref,
    q_ref,
    kv_ref,
    cos_ref,
    sin_ref,
    gain_ref,
    w_ref,
    out_ref,
    kv_all,
    w_all,
    heads_all,
    built,
    own_sem,
    kv_send,
    kv_recv,
    w_send,
    w_recv,
    x_send,
    x_recv,
    mate_send,
    mate_recv,
    out_send,
    out_recv,
):
    bf16 = jnp.bfloat16
    d = lax.axis_index("dp")
    me = lax.axis_index("sp")
    half = count // 2
    tall = n // half
    steps = n // 2
    width = 2 * HEAD_DIM
    rows = q_ref.shape[0]
    seqlen = n * rows

    def flip(column, place):
        return place + column % 2 * (tall - 1 - 2 * place)

    pos = me % half * tall + flip(me % half, me // half)

    def at(place):
        place = (place + 2 * n) % n
        column = place // tall
        return flip(column, place % tall) * half + column

    ahead, behind = at(pos + 1), at(pos - 1)
    x, core = d // 2, d % 2
    mate = x * 2 + 1 - core

    def peer(k):
        return (x + k) % half * 2 + core

    barrier = pltpu.get_barrier_semaphore()
    for other in (ahead, behind):
        pl.semaphore_signal(barrier, inc=1, device_id={"sp": other}, device_id_type=MESH)
    for k in range(1, count):
        pl.semaphore_signal(barrier, inc=1, device_id={"dp": (d + k) % count}, device_id_type=MESH)
    pl.semaphore_wait(barrier, count + 1)

    def ring_step(own, held, sends, recvs, t):
        pair = []
        for way in range(2):
            slot = at(pos - (t - 1)) if way == 0 else at(pos + (t - 1))
            src = own if t == 1 else held.at[slot]
            dst = held.at[slot]
            if t == steps:
                cut = held.shape[1] // 2
                part = pl.ds(way * cut, cut)
                src, dst = src.at[part], dst.at[part]
            pair.append(
                send(src, dst, sends.at[way, t - 1], recvs.at[way, t - 1], "sp", behind if way else ahead)
            )
            pair[-1].start()
        return pair

    kv_pairs = [ring_step(kv_ref, kv_all, kv_send, kv_recv, 1)]
    local = pltpu.make_async_copy(kv_ref, kv_all.at[me], own_sem)
    local.start()
    w_pairs = []
    for t in range(1, steps + 1):
        for copy in kv_pairs[t - 1]:
            copy.wait_recv()
        if t < steps:
            kv_pairs.append(ring_step(kv_ref, kv_all, kv_send, kv_recv, t + 1))
        if t == steps - 1:
            w_pairs.append(ring_step(w_ref, w_all, w_send, w_recv, 1))
    local.wait()

    allowed = lax.broadcasted_iota(jnp.int32, (rows, seqlen), 1) <= (
        me * rows + lax.broadcasted_iota(jnp.int32, (rows, seqlen), 0)
    )
    lane = lax.broadcasted_iota(jnp.int32, (rows, width), 1)

    def span(g):
        return pl.ds(pl.multiple_of(g * GROUP * VALUE_DIM, GROUP * VALUE_DIM), GROUP * VALUE_DIM)

    def sends_of(g):
        part = heads_all.at[d, :, span(g)]
        result = [send(part, part, x_send.at[0, g], x_recv.at[0, g], "dp", mate)]
        for k in range(1, half):
            result.append(send(part, part, x_send.at[k, g], x_recv.at[k, g], "dp", peer(k)))
        return result

    def one_group(g, carry):
        key = kv_all[:, :, pl.ds(pl.multiple_of(g * width, width), width)]
        key = key.reshape(seqlen, width)
        start = pl.multiple_of(KV_HEADS * width + g * VALUE_DIM, VALUE_DIM)
        value = kv_all[:, :, pl.ds(start, VALUE_DIM)].reshape(seqlen, VALUE_DIM)
        for h in range(GROUP):
            column = pl.multiple_of((g * GROUP + h) * width, width)
            query = q_ref[:, pl.ds(column, width)].astype(jnp.float32)
            query = turn(query, cos_ref[...], sin_ref[...]).astype(bf16)
            query = query.astype(jnp.float32) * HEAD_DIM**-0.5
            maps = []
            for m in range(2):
                mine = (lane < HEAD_DIM) if m == 0 else (lane >= HEAD_DIM)
                part = jnp.where(mine, query, 0.0).astype(bf16)
                scores = lax.dot_general(
                    part, key, (((1,), (1,)), ((), ())), preferred_element_type=jnp.float32
                )
                scores = jnp.where(allowed, scores, -1e30)
                raised = jnp.exp(scores - jnp.max(scores, -1, keepdims=True))
                maps.append((raised, 1.0 / jnp.sum(raised, -1, keepdims=True)))
            lam = lam_ref[g * GROUP + h]
            weights = (
                maps[0][0] * maps[0][1] - maps[1][0] * (lam * maps[1][1])
            ).astype(bf16)
            found = jnp.dot(weights, value, preferred_element_type=jnp.float32)
            squares = jnp.mean(found * found, -1, keepdims=True)
            normed = found * lax.rsqrt(squares + norm_eps) * gain_ref[...] * output_scale
            heads_all[d, :, pl.ds(column, width)] = normed.astype(bf16)
        for copy in sends_of(g):
            copy.start()
        return carry

    lax.fori_loop(0, KV_HEADS, one_group, 0)

    def weights_step(t):
        for copy in w_pairs[t - 1]:
            copy.wait_recv()
        if t < steps:
            w_pairs.append(ring_step(w_ref, w_all, w_send, w_recv, t + 1))

    weights_step(1)

    forwards = []
    for g in range(KV_HEADS):
        copies = sends_of(g)
        for k in range(1, half):
            copies[k].wait_recv()
            part = heads_all.at[(x + half - k) % half * 2 + core, :, span(g)]
            forwards.append(
                send(part, part, mate_send.at[k, g], mate_recv.at[k, g], "dp", mate)
            )
            forwards[-1].start()
    for g in range(KV_HEADS):
        sends_of(g)[0].wait_recv()
    for copy in forwards:
        copy.wait_recv()

    heads = heads_all[...].reshape(count * rows, heads_all.shape[2])
    own = w_ref.shape[1]
    outs = []
    for t in range(1, steps + 1):
        if t > 1:
            weights_step(t)
        places = (pos - t, pos + t) if t < steps else (pos, pos + steps)
        slots = [at(place) for place in places]
        blocks = [
            w_ref[...] if t == steps and i == 0 else w_all[slots[i]] for i in range(2)
        ]
        if own % 128 == 0:
            both = jnp.concatenate(blocks, -1)
            both = jnp.dot(heads, both, preferred_element_type=jnp.float32).astype(bf16)
            results = [both[:, :own], both[:, own:]]
        else:
            results = [
                jnp.dot(heads, block, preferred_element_type=jnp.float32).astype(bf16)
                for block in blocks
            ]
        for i in range(2):
            built[t - 1, i] = results[i].reshape(count, rows, own)
        for k in range(1, count):
            to = (d + k) % count
            for i in range(2):
                outs.append(
                    send(
                        built.at[t - 1, i, to],
                        out_ref.at[slots[i], d],
                        out_send.at[t - 1, i, k],
                        out_recv.at[t - 1, i, k],
                        "dp",
                        to,
                    )
                )
                outs[-1].start()
        for i in range(2):
            out_ref[slots[i], d] = built[t - 1, i, d]
    for copy in outs:
        copy.wait()
    for pair in kv_pairs + w_pairs:
        for copy in pair:
            copy.wait_send()
    for g in range(KV_HEADS):
        for copy in sends_of(g):
            copy.wait_send()
    for copy in forwards:
        copy.wait_send()


def lay_kernel(in_ref, out_ref):
    own = in_ref.shape[2]
    for b in range(in_ref.shape[0]):
        out_ref[:, b * own : (b + 1) * own] = in_ref[b]


def shards(queries, keys, values, lambdas, value_gain, out_weight):
    rows = queries.shape[1]
    sp_count = lax.axis_size("sp")
    dp_count = lax.axis_size("dp")
    width = 2 * HEAD_DIM
    vmem = pl.BlockSpec(memory_space=pltpu.VMEM)
    bf16 = jnp.bfloat16
    positions = (lax.axis_index("sp") * rows + jnp.arange(rows)).astype(jnp.float32)
    cosine, sine = tables(positions)
    kv_width = 2 * KV_HEADS * width

    kv = pl.pallas_call(
        prep_kernel,
        out_shape=jax.ShapeDtypeStruct((rows, kv_width), bf16),
        in_specs=[vmem] * 4,
        out_specs=vmem,
        name="prep",
    )(keys[0], values[0], cosine, sine)

    half = dp_count // 2
    steps = sp_count // 2
    depth, own = out_weight.shape
    dma = pltpu.SemaphoreType.DMA
    mixed = pl.pallas_call(
        functools.partial(layer_kernel, sp_count, dp_count),
        out_shape=jax.ShapeDtypeStruct((sp_count, dp_count, rows, own), bf16),
        in_specs=[pl.BlockSpec(memory_space=pltpu.SMEM)] + [vmem] * 6,
        out_specs=vmem,
        scratch_shapes=[
            pltpu.VMEM((sp_count, rows, kv_width), bf16),
            pltpu.VMEM((sp_count, depth, own), bf16),
            pltpu.VMEM((dp_count, rows, depth), bf16),
            pltpu.VMEM((steps, 2, dp_count, rows, own), bf16),
            dma(()),
        ]
        + [dma((2, steps))] * 4
        + [dma((half, KV_HEADS))] * 4
        + [dma((steps, 2, dp_count))] * 2,
        compiler_params=pltpu.CompilerParams(
            collective_id=0, has_side_effects=True, vmem_limit_bytes=60 * 2**20
        ),
        name="layer",
    )(lambdas, queries[0], kv, cosine, sine, value_gain[None], out_weight)

    if own % 128 == 0:
        return pl.pallas_call(
            lay_kernel,
            out_shape=jax.ShapeDtypeStruct((rows, sp_count * dp_count * own), bf16),
            in_specs=[vmem],
            out_specs=vmem,
            name="lay",
        )(mixed.reshape(-1, rows, own))[None]
    return jnp.transpose(mixed, (2, 0, 1, 3)).reshape(1, rows, -1)


def solution(mesh):
    return jax.shard_map(
        shards,
        mesh=mesh,
        in_specs=(
            P("dp", "sp", None),
            P("dp", "sp", None),
            P("dp", "sp", None),
            P(),
            P(),
            P(None, ("sp", "dp")),
        ),
        out_specs=P("dp", "sp", None),
        check_vma=False,
    )
```

time: 164 us -> 83.6 us (0.51)
  waiting for transfers between devices: 93.9 us -> 0 us
  Pallas kernels: 51 us -> 82.3 us
  between operations: 13.4 us -> 0.02 us
  local copies, waits for them, and re-layouts: 4.31 us -> 0 us
    all_gather x2 -> x0, waiting for transfers between devices: 93.8 us -> none  [the longest x1 51.9 us: shards(): kv_whole = lax.all_gather(kv, 'sp', axis=0, tiled=True)]
    pallas_call x4 -> x3, Pallas kernels: 51 us -> 82.3 us  [the longest x1 78 us: shards(): pl.pallas_call(functools.partial(layer_kernel, sp_count, dp_count), out_s...]
    reshape x2 -> x0, local copies, waits for them, and re-layouts: 2.95 us -> none  [the longest x1 1.61 us: shards(): return mixed.reshape(1, rows, -1)]
  transfers between devices with their start and end apart: 2 -> 0, of which waited for: 2 -> 0; matrix products, arithmetic and copies ran while one was open for 0% -> 0% of each run, Pallas kernels for 19% -> 0%
where the time goes in v2:
time: 83.6 us; the launch traced here: 83.5 us
  Pallas kernels  82.3 us (98%)
  other arithmetic  1.15 us (1%)
    pallas_call x1, Pallas kernels, shards(): pl.pallas_call(functools.partial(layer_kernel, sp_count, dp_count), out_s...  78 us
    pallas_call x1, Pallas kernels, shards(): pl.pallas_call(lay_kernel, out_shape=jax.ShapeDtypeStruct((rows, sp_count...  2.47 us
    pallas_call x1, Pallas kernels, shards(): pl.pallas_call(prep_kernel, out_shape=jax.ShapeDtypeStruct((rows, kv_widt...  1.85 us

profile of v2, /device:TPU:0, one launch (start us, length us, event | category | flops | bytes accessed | tf_op | source)
XLA Modules:
  0.0 83.5 jit_solution(6772512420847091071)
XLA Ops:
  0.0 0.3 fusion
  0.3 0.8 pad_maximum_fusion
  1.2 1.8 %prep.1.kv_ref = bf16[128,1024]{1,0:T(8,128)(2,1)} custom-call(bf16[128,512]{1,0:T(8,128)(2,1)} %bitcast.8, bf16[128,512]{1,0:T(8,128)(2,1)} %bitcast.9, f32[128,128]{1,0:T(8,128)} %get-tuple-element.8.cos_ref, f32[128,128]{1,0:T(8,128)} %get-tuple-element.9.sin_ref), custom_call_target="tpu_custom_call" | custom-call | tf_op jit(solution)/shard_map/prep/pallas_call | solution.py:290
  3.0 78.0 %layer.1 = bf16[8,4,128,128]{3,2,1,0:T(8,128)(2,1)} custom-call(f32[16]{0:T(128)} %lam_ref.1, bf16[128,2048]{1,0:T(8,128)(2,1)} %bitcast.7, bf16[128,1024]{1,0:T(8,128)(2,1)} %prep.1.kv_ref, f32[128,128]{1,0:T(8,128)} %get-tuple-element.8.cos_ref, f32[128,128]{1,0:T(8,128)} %get-tuple-element.9.sin_ref, f32[1,128]{1,0:T(1,128)} %bitcast.10, ...), custom_call_target="tpu_custom_call" | custom-call | tf_op jit(solution)/shard_map/layer/pallas_call | solution.py:302
  81.0 2.5 %lay.1 = bf16[128,4096]{1,0:T(8,128)(2,1)} custom-call(bf16[32,128,128]{2,1,0:T(8,128)(2,1)} %bitcast.6), custom_call_target="tpu_custom_call" | custom-call | tf_op jit(solution)/shard_map/lay/pallas_call | solution.py:324
  (2 shorter events, 0.0 us)

commit v3 on v2

--- a/solution.py
+++ b/solution.py
@@ -37,16 +37,6 @@
     return block * cosine + other * sine
 
 
-def prep_kernel(k_ref, v_ref, cos_ref, sin_ref, kv_ref):
-    width = 2 * HEAD_DIM
-    for g in range(KV_HEADS):
-        cols = slice(g * width, (g + 1) * width)
-        kv_ref[:, cols] = turn(
-            k_ref[:, cols].astype(jnp.float32), cos_ref[...], sin_ref[...]
-        ).astype(jnp.bfloat16)
-    kv_ref[:, KV_HEADS * width :] = v_ref[...]
-
-
 def send(src, dst, send_sem, recv_sem, axis, index):
     return pltpu.make_async_remote_copy(
         src_ref=src,
@@ -63,12 +53,14 @@
     count,
     lam_ref,
     q_ref,
-    kv_ref,
+    k_ref,
+    v_ref,
     cos_ref,
     sin_ref,
     gain_ref,
     w_ref,
     out_ref,
+    kv_own,
     kv_all,
     w_all,
     heads_all,
@@ -117,36 +109,61 @@
         pl.semaphore_signal(barrier, inc=1, device_id={"sp": other}, device_id_type=MESH)
     for k in range(1, count):
         pl.semaphore_signal(barrier, inc=1, device_id={"dp": (d + k) % count}, device_id_type=MESH)
+    for g in range(KV_HEADS):
+        cols = slice(g * width, (g + 1) * width)
+        key = turn(k_ref[:, cols].astype(jnp.float32), cos_ref[...], sin_ref[...])
+        kv_own[:, cols] = key.astype(bf16)
+    kv_own[:, KV_HEADS * width :] = v_ref[...]
     pl.semaphore_wait(barrier, count + 1)
 
-    def ring_step(own, held, sends, recvs, t):
-        pair = []
-        for way in range(2):
+    def ring_step(own, held, sends, recvs, t, p):
+        cut = held.shape[1] // 2
+        part = pl.ds(p * cut, cut)
+        copies = []
+        for way in range(2) if t < steps else (p,):
             slot = at(pos - (t - 1)) if way == 0 else at(pos + (t - 1))
-            src = own if t == 1 else held.at[slot]
-            dst = held.at[slot]
-            if t == steps:
-                cut = held.shape[1] // 2
-                part = pl.ds(way * cut, cut)
-                src, dst = src.at[part], dst.at[part]
-            pair.append(
-                send(src, dst, sends.at[way, t - 1], recvs.at[way, t - 1], "sp", behind if way else ahead)
+            dst = held.at[slot].at[part]
+            copies.append(
+                send(
+                    own.at[part] if t == 1 else dst,
+                    dst,
+                    sends.at[way, t - 1, p],
+                    recvs.at[way, t - 1, p],
+                    "sp",
+                    behind if way else ahead,
+                )
             )
-            pair[-1].start()
-        return pair
-
-    kv_pairs = [ring_step(kv_ref, kv_all, kv_send, kv_recv, 1)]
-    local = pltpu.make_async_copy(kv_ref, kv_all.at[me], own_sem)
+            copies[-1].start()
+        return copies
+
+    kv_copies, w_copies = {}, {}
+
+    def kv_step(t, p):
+        kv_copies[t, p] = ring_step(kv_own, kv_all, kv_send, kv_recv, t, p)
+
+    def w_step(t, p):
+        w_copies[t, p] = ring_step(w_ref, w_all, w_send, w_recv, t, p)
+
+    kv_step(1, 0)
+    kv_step(1, 1)
+    local = pltpu.make_async_copy(kv_own, kv_all.at[me], own_sem)
     local.start()
-    w_pairs = []
     for t in range(1, steps + 1):
-        for copy in kv_pairs[t - 1]:
+        for p in range(2):
+            for copy in kv_copies[t, p]:
+                copy.wait_recv()
+            if t < steps:
+                kv_step(t + 1, p)
+        if t == steps - 1:
+            w_step(1, 0)
+            w_step(1, 1)
+    local.wait()
+
+    def w_relay(t, p):
+        for copy in w_copies[t, p]:
             copy.wait_recv()
         if t < steps:
-            kv_pairs.append(ring_step(kv_ref, kv_all, kv_send, kv_recv, t + 1))
-        if t == steps - 1:
-            w_pairs.append(ring_step(w_ref, w_all, w_send, w_recv, 1))
-    local.wait()
+            w_step(t + 1, p)
 
     allowed = lax.broadcasted_iota(jnp.int32, (rows, seqlen), 1) <= (
         me * rows + lax.broadcasted_iota(jnp.int32, (rows, seqlen), 0)
@@ -195,15 +212,10 @@
             copy.start()
         return carry
 
-    lax.fori_loop(0, KV_HEADS, one_group, 0)
-
-    def weights_step(t):
-        for copy in w_pairs[t - 1]:
-            copy.wait_recv()
-        if t < steps:
-            w_pairs.append(ring_step(w_ref, w_all, w_send, w_recv, t + 1))
-
-    weights_step(1)
+    lax.fori_loop(0, KV_HEADS // 2, one_group, 0)
+    w_relay(1, 0)
+    lax.fori_loop(KV_HEADS // 2, KV_HEADS, one_group, 0)
+    w_relay(1, 1)
 
     forwards = []
     for g in range(KV_HEADS):
@@ -223,45 +235,48 @@
     heads = heads_all[...].reshape(count * rows, heads_all.shape[2])
     own = w_ref.shape[1]
     outs = []
-    for t in range(1, steps + 1):
-        if t > 1:
-            weights_step(t)
-        places = (pos - t, pos + t) if t < steps else (pos, pos + steps)
+
+    def project(index, places):
         slots = [at(place) for place in places]
-        blocks = [
-            w_ref[...] if t == steps and i == 0 else w_all[slots[i]] for i in range(2)
-        ]
+        blocks = [w_all[slot] if index else w_ref[...] for slot in slots]
         if own % 128 == 0:
-            both = jnp.concatenate(blocks, -1)
+            both = jnp.concatenate(blocks, -1) if len(blocks) > 1 else blocks[0]
             both = jnp.dot(heads, both, preferred_element_type=jnp.float32).astype(bf16)
-            results = [both[:, :own], both[:, own:]]
+            results = [both[:, i * own : (i + 1) * own] for i in range(len(blocks))]
         else:
             results = [
                 jnp.dot(heads, block, preferred_element_type=jnp.float32).astype(bf16)
                 for block in blocks
             ]
-        for i in range(2):
-            built[t - 1, i] = results[i].reshape(count, rows, own)
+        for i in range(len(slots)):
+            built[index, i] = results[i].reshape(count, rows, own)
         for k in range(1, count):
             to = (d + k) % count
-            for i in range(2):
+            for i in range(len(slots)):
                 outs.append(
                     send(
-                        built.at[t - 1, i, to],
+                        built.at[index, i, to],
                         out_ref.at[slots[i], d],
-                        out_send.at[t - 1, i, k],
-                        out_recv.at[t - 1, i, k],
+                        out_send.at[index, i, k],
+                        out_recv.at[index, i, k],
                         "dp",
                         to,
                     )
                 )
                 outs[-1].start()
-        for i in range(2):
-            out_ref[slots[i], d] = built[t - 1, i, d]
+        for i in range(len(slots)):
+            out_ref[slots[i], d] = built[index, i, d]
+
+    project(0, (pos,))
+    for t in range(1, steps + 1):
+        if t > 1:
+            w_relay(t, 0)
+            w_relay(t, 1)
+        project(t, (pos - t, pos + t) if t < steps else (pos + t,))
     for copy in outs:
         copy.wait()
-    for pair in kv_pairs + w_pairs:
-        for copy in pair:
+    for copies in list(kv_copies.values()) + list(w_copies.values()):
+        for copy in copies:
             copy.wait_send()
     for g in range(KV_HEADS):
         for copy in sends_of(g):
@@ -287,14 +302,6 @@
     cosine, sine = tables(positions)
     kv_width = 2 * KV_HEADS * width
 
-    kv = pl.pallas_call(
-        prep_kernel,
-        out_shape=jax.ShapeDtypeStruct((rows, kv_width), bf16),
-        in_specs=[vmem] * 4,
-        out_specs=vmem,
-        name="prep",
-    )(keys[0], values[0], cosine, sine)
-
     half = dp_count // 2
     steps = sp_count // 2
     depth, own = out_weight.shape
@@ -302,23 +309,24 @@
     mixed = pl.pallas_call(
         functools.partial(layer_kernel, sp_count, dp_count),
         out_shape=jax.ShapeDtypeStruct((sp_count, dp_count, rows, own), bf16),
-        in_specs=[pl.BlockSpec(memory_space=pltpu.SMEM)] + [vmem] * 6,
+        in_specs=[pl.BlockSpec(memory_space=pltpu.SMEM)] + [vmem] * 7,
         out_specs=vmem,
         scratch_shapes=[
+            pltpu.VMEM((rows, kv_width), bf16),
             pltpu.VMEM((sp_count, rows, kv_width), bf16),
             pltpu.VMEM((sp_count, depth, own), bf16),
             pltpu.VMEM((dp_count, rows, depth), bf16),
-            pltpu.VMEM((steps, 2, dp_count, rows, own), bf16),
+            pltpu.VMEM((steps + 1, 2, dp_count, rows, own), bf16),
             dma(()),
         ]
-        + [dma((2, steps))] * 4
+        + [dma((2, steps, 2))] * 4
         + [dma((half, KV_HEADS))] * 4
-        + [dma((steps, 2, dp_count))] * 2,
+        + [dma((steps + 1, 2, dp_count))] * 2,
         compiler_params=pltpu.CompilerParams(
             collective_id=0, has_side_effects=True, vmem_limit_bytes=60 * 2**20
         ),
         name="layer",
-    )(lambdas, queries[0], kv, cosine, sine, value_gain[None], out_weight)
+    )(lambdas, queries[0], keys[0], values[0], cosine, sine, value_gain[None], out_weight)
 
     if own % 128 == 0:
         return pl.pallas_call(

time: 83.6 us -> 80.4 us (0.962)
  Pallas kernels: 82.3 us -> 79.1 us
    pallas_call x1 -> x0, Pallas kernels: 1.85 us -> none  [shards(): pl.pallas_call(prep_kernel, out_shape=jax.ShapeDtypeStruct((rows, kv_widt...]
    pallas_call x1, Pallas kernels: 78 us -> 76.6 us  [shards(): pl.pallas_call(functools.partial(layer_kernel, sp_count, dp_count), out_s...]
where the time goes in v3:
time: 80.4 us; the launch traced here: 80.2 us
  Pallas kernels  79.1 us (98%)
  other arithmetic  1.15 us (1%)
    pallas_call x1, Pallas kernels, shards(): pl.pallas_call(functools.partial(layer_kernel, sp_count, dp_count), out_s...  76.6 us
    pallas_call x1, Pallas kernels, shards(): pl.pallas_call(lay_kernel, out_shape=jax.ShapeDtypeStruct((rows, sp_count...  2.47 us

profile of v3, /device:TPU:0, one launch (start us, length us, event | category | flops | bytes accessed | tf_op | source)
XLA Modules:
  0.0 80.2 jit_solution(11524615417130204042)
XLA Ops:
  0.0 0.3 fusion
  0.3 0.8 %pad_maximum_fusion = (f32[128,128]{1,0:T(8,128)}, f32[128,128]{1,0:T(8,128)}) fusion(f32[128,32]{1,0:T(8,128)S(1)} %get-tuple-element.7, f32[128,32]{1,0:T(8,128)S(1)} %get-tuple-element.6, f32[128,32]{1,0:T(8,128)S(1)} %get-tuple-element.5), kind=kLoop, calls=%fused_computation.2 | loop fusion | flops 98304 | bytes 180224 | tf_op jit(solution)/shard_map/concatenate | solution.py:26
  1.2 76.6 %layer.1 = bf16[8,4,128,128]{3,2,1,0:T(8,128)(2,1)} custom-call(f32[16]{0:T(128)} %lam_ref.1, bf16[128,2048]{1,0:T(8,128)(2,1)} %bitcast.7, bf16[128,512]{1,0:T(8,128)(2,1)} %bitcast.8, bf16[128,512]{1,0:T(8,128)(2,1)} %bitcast.9, f32[128,128]{1,0:T(8,128)} %get-tuple-element.8.cos_ref, f32[128,128]{1,0:T(8,128)} %get-tuple-element.9.sin_ref, ...), custom_call_target="tpu_custom_call" | custom-call | tf_op jit(solution)/shard_map/layer/pallas_call | solution.py:309
  77.8 2.5 %lay.1 = bf16[128,4096]{1,0:T(8,128)(2,1)} custom-call(bf16[32,128,128]{2,1,0:T(8,128)(2,1)} %bitcast.6), custom_call_target="tpu_custom_call" | custom-call | tf_op jit(solution)/shard_map/lay/pallas_call | solution.py:332
  (2 shorter events, 0.0 us)
